TPU v7x, 32 devices: a whole 2x2x4 slice. The times are simulated.
32 devices in a mesh: ep: 8 (over z, x), tp: 4 (over y, core).
Axes of the slice: x: 2, y: 2, z: 4, core: 2. Of those that a mesh axis runs over, the one named last changes fastest.
Arguments:
- mix_query: bfloat16 [2048, 2048], P('ep', 'tp'), may hold values from -6 to 6
- forget_input: bfloat16 [2048, 2048], P('ep', 'tp'), may hold values from -6 to 6
- mix_value: bfloat16 [2048, 2048], P('ep', 'tp'), may hold values from -6 to 6
- out_gate_input: bfloat16 [2048, 2048], P('ep', 'tp'), may hold values from -6 to 6
- decay_shift: float32 [2048, 16], P('ep', 'tp'), may hold values from -1.5 to 0
- forget_floor: float32 [2048], P('tp'), may hold values from 0.9 to 1
- head_gain: float32 [128], replicated, may hold values from 0.1 to 1.9
- w_mix_out: bfloat16 [2048, 2048], P(None, 'tp'), may hold values from -0.125 to 0.125
- moe_input: bfloat16 [2048, 2048], P('ep'), may hold values from -6 to 6
- moe_gain: float32 [2048], replicated, may hold values from 0.1 to 1.9
- routes: int32 [2048, 2], P('ep'), may hold values from 0 to 7, all different within a row; in each aligned block of 256 rows (0 to 255, 256 to 511, ...) at most 80 rows name the same one
- route_weight: float32 [2048, 2], P('ep'), may hold values from 0.1 to 1
- w_exp_gate: bfloat16 [8, 2048, 4096], P('ep', None, 'tp'), may hold values from -0.125 to 0.125
- w_exp_up: bfloat16 [8, 2048, 4096], P('ep', None, 'tp'), may hold values from -0.125 to 0.125
- w_exp_down: bfloat16 [8, 4096, 2048], P('ep', 'tp'), may hold values from -0.125 to 0.125
Outputs:
- mixed: bfloat16 [2048, 2048], P('ep', 'tp')
- moe_out: bfloat16 [2048, 2048], P('ep', 'tp')
Inputs may be any that keep to these rules, and one draw needn't show every extreme that they name: `routes`: at most 80 of the rows of one index of ep name one expert, and in every draw some device's rows name one expert exactly 80 times; the experts of a row differ.
All inputs are finite; a program needn't handle non-finite values.
Results may differ from a plain program's by a relative error of at most 0.02.
Values may be sent and summed in bfloat16 or wider, within the bound.
A program may use at most 64 MiB of HBM per device.

v0:
```python
import functools

import jax
import jax.numpy as jnp
from jax import lax
from jax.experimental import pallas as pl
from jax.experimental.pallas import tpu as pltpu
from jax.sharding import PartitionSpec as P

TOP_K = 2
EPS = 1e-06
MESH = pl.DeviceIdType.MESH
BF = jnp.bfloat16
F32 = jnp.float32
HIGH = lax.Precision.HIGHEST


def mm(a, b, dims=((1,), (0,)), precision=None):
    return lax.dot_general(
        a, b, (dims, ((), ())), preferred_element_type=F32, precision=precision
    )


def scan_windows(ep):
    windows = [0]
    w = 1
    while w < ep - 1:
        windows.append(w)
        w *= 2
    return windows


def kernel(
    cfg,
    q_ref,
    fi_ref,
    v_ref,
    og_ref,
    ds_ref,
    ff_ref,
    hg_ref,
    x_ref,
    mg_ref,
    rt_ref,
    rw_ref,
    wm_hbm,
    wg_hbm,
    wu_hbm,
    wd_hbm,
    mixed_ref,
    moe_ref,
    wm,
    wg,
    wu,
    wd,
    disp,
    xs,
    hid,
    snd_p,
    rs_p,
    own,
    snd_y,
    rs_y,
    fin,
    ret,
    pick,
    ks_s,
    ks_r,
    carry,
    intra,
    qdec,
    ho,
    w_sem,
    a_ss,
    a_rs,
    gy_ss,
    gy_rs,
    gp_ss,
    gp_rs,
    rp_ss,
    rp_rs,
    ry_ss,
    ry_rs,
    b_ss,
    b_rs,
    k_ss,
    k_rs,
    hy_ss,
    hy_rs,
    hp_ss,
    hp_rs,
):
    ep, tp, cap, groups = cfg
    gb = ep // groups
    ny = tp // 2
    me = lax.axis_index("ep")
    t = lax.axis_index("tp")
    y = t // 2
    c = t % 2
    mate = y * 2 + (1 - c)
    rows, dim = x_ref.shape
    width = dim // tp
    slots = ep * cap
    hidden_units = wg.shape[1]
    heads = ds_ref.shape[0]
    hs = hg_ref.shape[1]
    hw = q_ref.shape[1]

    def ring(a, n):
        return lax.rem(a + n, n)

    def up_y(dy):
        return ring(y + dy, ny)

    def dn_y(dy):
        return ring(y - dy, ny)

    def rc(src, dst, ss, rs, e, j):
        return pltpu.make_async_remote_copy(
            src_ref=src, dst_ref=dst, send_sem=ss, recv_sem=rs, device_id=(e, j), device_id_type=MESH
        )

    loads = [
        pltpu.make_async_copy(wg_hbm.at[0], wg, w_sem.at[0]),
        pltpu.make_async_copy(wu_hbm.at[0], wu, w_sem.at[1]),
        pltpu.make_async_copy(wd_hbm.at[0], wd, w_sem.at[2]),
        pltpu.make_async_copy(wm_hbm, wm, w_sem.at[3]),
    ]
    barrier = pltpu.get_barrier_semaphore()
    for d in range(1, ep):
        pl.semaphore_signal(barrier, inc=1, device_id=(ring(me + d, ep), t), device_id_type=MESH)
    for dy in range(1, ny):
        pl.semaphore_signal(barrier, inc=1, device_id=(me, up_y(dy) * 2 + c), device_id_type=MESH)
    pl.semaphore_signal(barrier, inc=1, device_id=(me, mate), device_id_type=MESH)
    for load in loads:
        load.start()

    i_r = lax.broadcasted_iota(jnp.int32, (rows, rows), 0)
    i_c = lax.broadcasted_iota(jnp.int32, (rows, rows), 1)
    lane = lax.broadcasted_iota(jnp.int32, (rows, 128), 1)
    slot_lane = lax.broadcasted_iota(jnp.int32, (rows, slots), 1)
    eye = (i_r == i_c).astype(F32)
    ids = mm(eye, rt_ref[...].astype(F32), ((1,), (1,)), HIGH).astype(jnp.int32)
    rel, hot = [], []
    for k in range(TOP_K):
        e = ids[:, k : k + 1]
        r = jnp.where(e >= me, e - me, e - me + ep)
        rel.append(r)
        hot.append((lane == r).astype(F32))
    before = mm((i_r > i_c).astype(F32).astype(BF), sum(hot).astype(BF))
    both = None
    for k in range(TOP_K):
        rank = jnp.sum(before * hot[k], axis=1, keepdims=True).astype(jnp.int32)
        p = (slot_lane == rel[k] * cap + rank).astype(F32)
        both = p if both is None else both + p
        pick[k] = p.astype(BF)
    xf = x_ref[...].astype(F32)
    inv = lax.rsqrt(jnp.mean(xf * xf, axis=1, keepdims=True) + EPS)
    cols = pl.ds(pl.multiple_of(t * width, width), width)
    normed = (x_ref[:, cols].astype(F32) * inv * mg_ref[:, cols]).astype(BF)
    out = mm(both.astype(BF), normed, ((0,), (0,))).astype(BF).reshape(ep, cap, width)
    disp[...] = out
    xs[t, 0] = out[0]

    pl.semaphore_wait(barrier, ep - 1 + ny)

    def a2a(d):
        return rc(disp.at[d], xs.at[t, d], a_ss.at[d], a_rs.at[d], ring(me + d, ep), t)

    for d in range(1, ep):
        a2a(d).start()

    def gat(col, g):
        return xs.at[col, pl.ds(g * gb, gb)]

    def gat_y(g, dy):
        r = gat(t, g)
        return rc(r, r, gy_ss.at[g, dy], gy_rs.at[g, dy], me, up_y(dy) * 2 + c)

    def gat_y_in(g, dy):
        r = gat(dn_y(dy) * 2 + c, g)
        return rc(r, r, gy_ss.at[g, dy], gy_rs.at[g, dy], me, mate)

    def gat_p(g, dy):
        r = gat(dn_y(dy) * 2 + c, g)
        return rc(r, r, gp_ss.at[g, dy], gp_rs.at[g, dy], me, mate)

    def gat_p_in(g, dy):
        r = gat(dn_y(dy) * 2 + 1 - c, g)
        return rc(r, r, gp_ss.at[g, dy], gp_rs.at[g, dy], me, mate)

    def relay1(g):
        for d in range(max(1, g * gb), (g + 1) * gb):
            a2a(d).wait_recv()
        for dy in range(1, ny):
            gat_y(g, dy).start()
        gat_p(g, 0).start()

    def relay2(g):
        for dy in range(1, ny):
            gat_y_in(g, dy).wait_recv()
            gat_p(g, dy).start()

    def arrived(g):
        for dy in range(ny):
            gat_p_in(g, dy).wait_recv()

    causal = i_r >= i_c
    tri = causal.astype(F32)

    def mix_all_decay():
        fl = ff_ref[...]
        fx = fi_ref[...].astype(F32)
        forget = fl + (1.0 - fl) * jax.nn.sigmoid(fx)
        return mm(tri, jnp.log(forget), precision=HIGH)

    def mix_head(h, run, s_col, s_row):
        hc = slice(h * hs, (h + 1) * hs)
        lr = run[:, hc]
        sc = s_col[:, h : h + 1]
        sr = s_row[h : h + 1, :]
        key = (1.0 - ff_ref[:, hc]) * jax.nn.sigmoid(-fi_ref[:, hc].astype(F32))
        q = q_ref[:, hc].astype(F32) * jnp.exp(lr)
        v = v_ref[:, hc]
        scores = mm(q.astype(BF), (key * jnp.exp(-lr)).astype(BF), ((1,), (1,)))
        scores = jnp.where(causal, scores * jnp.exp(jnp.minimum(sc - sr, 0.0)), 0.0)
        intra[:, hc] = mm(scores.astype(BF), v)
        qdec[:, hc] = (q * jnp.exp(sc)).astype(BF)
        l_end = lr[rows - 1 : rows, :]
        s_end = sc[rows - 1 : rows, :]
        kd = (key * jnp.exp(l_end - lr + (s_end - sc))).astype(BF)
        ks_s[0, h, 0:hs, :] = mm(v, kd, ((0,), (0,))).astype(BF)
        ks_s[0, h, hs : hs + 16, :] = jnp.broadcast_to(jnp.exp(l_end + s_end), (16, hs)).astype(BF)

    windows = scan_windows(ep)

    def scan_copy(i):
        hop = max(1, windows[i])
        return rc(ks_s.at[i], ks_r.at[i], k_ss.at[i], k_rs.at[i], ring(me + hop, ep), t)

    def scan_send(i, act):
        pl.when(me + max(1, windows[i]) < ep)(lambda: act(scan_copy(i)))

    def scan_take(i):
        hop = max(1, windows[i])
        have = me >= hop

        @pl.when(jnp.logical_not(have))
        def _():
            ks_r[i] = jnp.zeros(ks_r.shape[1:], BF)

        pl.when(have)(lambda: scan_copy(i).wait_recv())
        for h in range(heads):
            got = ks_r[i, h].astype(F32)
            s_in = jnp.where(have, got[0:hs], 0.0)
            a_in = jnp.where(have, got[hs : hs + 16], 1.0)
            if i > 0:
                a_own = carry[h, hs : hs + 16, :]
                s_in = a_own[0:1] * s_in + carry[h, 0:hs, :]
                a_in = a_own * a_in
            carry[h, 0:hs, :] = s_in
            carry[h, hs : hs + 16, :] = a_in
            if i + 1 < len(windows):
                ks_s[i + 1, h, 0:hs, :] = s_in.astype(BF)
                ks_s[i + 1, h, hs : hs + 16, :] = a_in.astype(BF)
        if i + 1 < len(windows):
            scan_send(i + 1, lambda a: a.start())

    def ho_y(dy):
        return rc(ho.at[t], ho.at[t], hy_ss.at[dy], hy_rs.at[dy], me, up_y(dy) * 2 + c)

    def ho_y_in(dy):
        r = ho.at[dn_y(dy) * 2 + c]
        return rc(r, r, hy_ss.at[dy], hy_rs.at[dy], me, mate)

    def ho_p(dy):
        r = ho.at[dn_y(dy) * 2 + c]
        return rc(r, r, hp_ss.at[dy], hp_rs.at[dy], me, mate)

    def ho_p_in(dy):
        r = ho.at[dn_y(dy) * 2 + 1 - c]
        return rc(r, r, hp_ss.at[dy], hp_rs.at[dy], me, mate)

    def mix_close():
        for h in range(heads):
            hc = slice(h * hs, (h + 1) * hs)
            o = intra[:, hc] + mm(qdec[:, hc], carry[h, 0:hs, :].astype(BF), ((1,), (1,)))
            iv = lax.rsqrt(jnp.mean(o * o, axis=1, keepdims=True) + EPS)
            g = og_ref[:, hc].astype(F32)
            ho[t, :, hc] = (o * iv * hg_ref[...] * (g * jax.nn.sigmoid(g))).astype(BF)
        for dy in range(1, ny):
            ho_y(dy).start()
        ho_p(0).start()

    def ho_relay():
        for dy in range(1, ny):
            ho_y_in(dy).wait_recv()
            ho_p(dy).start()

    gr = gb * cap
    ft = min(256, hidden_units)

    def first(g):
        def tile(n, _):
            fc = pl.ds(pl.multiple_of(n * ft, ft), ft)
            gate = jnp.zeros((gr, ft), F32)
            up = jnp.zeros((gr, ft), F32)
            for j in range(tp):
                a = xs[j, g * gb : (g + 1) * gb].reshape(gr, width)
                gate += mm(a, wg[j * width : (j + 1) * width, fc])
                up += mm(a, wu[j * width : (j + 1) * width, fc])
            hid[:, fc] = (gate * jax.nn.sigmoid(gate) * up).astype(BF)
            return 0

        lax.fori_loop(0, hidden_units // ft, tile, 0)

    def down(dy, core):
        col = up_y(dy) * 2 + core
        return mm(hid[...], wd[:, pl.ds(pl.multiple_of(col * width, width), width)])

    def red_p(g, dy):
        return rc(snd_p.at[g, dy], rs_p.at[g, dy], rp_ss.at[g, dy], rp_rs.at[g, dy], me, mate)

    def red_y(g, dy):
        return rc(
            snd_y.at[g, dy], rs_y.at[g, dy], ry_ss.at[g, dy], ry_rs.at[g, dy], me, up_y(dy) * 2 + c
        )

    order = list(range(1, ny)) + [0]

    def second(g):
        for dy in order:
            snd_p[g, dy] = down(dy, 1 - c).astype(BF)
            red_p(g, dy).start()
        for dy in order:
            own[g % 2, dy] = down(dy, c)
        for dy in order:
            red_p(g, dy).wait_recv()
            total = own[g % 2, dy] + rs_p[g, dy].astype(F32)
            if dy:
                snd_y[g, dy] = total.astype(BF)
                red_y(g, dy).start()
            else:
                own[g % 2, 0] = total

    def back(d):
        return rc(fin.at[d], ret.at[d], b_ss.at[d], b_rs.at[d], ring(me - d, ep), t)

    def third(g):
        total = own[g % 2, 0]
        for dy in range(1, ny):
            red_y(g, dy).wait_recv()
            total += rs_y[g, dy].astype(F32)
        blocks = total.astype(BF).reshape(gb, cap, width)
        for i in range(gb):
            d = g * gb + i
            if d == 0:
                ret[0] = blocks[0]
            else:
                fin[d] = blocks[i]
                back(d).start()

    run = mix_all_decay()
    s_col = mm(tri, ds_ref[...], ((1,), (1,)), HIGH)
    s_row = mm(ds_ref[...], tri, ((1,), (1,)), HIGH)
    for h in range(heads):
        mix_head(h, run, s_col, s_row)
        if h == heads // 2:
            relay1(0)
    scan_send(0, lambda a: a.start())
    relay1(1)
    relay2(0)
    scan_take(0)
    relay1(2)
    for load in loads[:3]:
        load.wait()
    taken = 1
    for g in range(groups):
        arrived(g)
        first(g)
        if g + 1 < groups:
            relay2(g + 1)
        if g + 3 < groups:
            relay1(g + 3)
        second(g)
        if taken < len(windows):
            scan_take(taken)
            taken += 1
        if g > 0:
            third(g - 1)
    while taken < len(windows):
        scan_take(taken)
        taken += 1
    mix_close()
    third(groups - 1)
    ho_relay()
    loads[3].wait()
    for dy in range(ny):
        ho_p_in(dy).wait_recv()
    acc = jnp.zeros(mixed_ref.shape, F32)
    for j in range(tp):
        acc += mm(ho[j], wm[j * hw : (j + 1) * hw, :])
    mixed_ref[...] = acc.astype(BF)
    for d in range(1, ep):
        back(d).wait_recv()
    flat = ret[...].reshape(slots, width)
    res = jnp.zeros(moe_ref.shape, F32)
    weight = mm(eye, rw_ref[...], ((1,), (1,)), HIGH)
    for k in range(TOP_K):
        res += mm(pick[k], flat) * weight[:, k : k + 1]
    moe_ref[...] = res.astype(BF)

    for d in range(1, ep):
        a2a(d).wait_send()
        back(d).wait_send()
    for i in range(len(windows)):
        scan_send(i, lambda a: a.wait_send())
    for dy in range(ny):
        ho_p(dy).wait_send()
        if dy:
            ho_y(dy).wait_send()
        for g in range(groups):
            gat_p(g, dy).wait_send()
            red_p(g, dy).wait_send()
            if dy:
                gat_y(g, dy).wait_send()
                red_y(g, dy).wait_send()


def emit(a_ref, b_ref, a_out, b_out):
    a_out[...] = a_ref[...]
    b_out[...] = b_ref[...]


def body(ep, tp, *args):
    (q, fi, v, og, ds, ff, hg, wm, x, mg, rt, rw, wg, wu, wd) = args
    rows, dim = x.shape
    capacity = 5 * rows * TOP_K // (4 * ep)
    cap = -(-capacity // 16) * 16
    groups = 4
    gb = ep // groups
    ny = tp // 2
    width = dim // tp
    heads = ds.shape[1]
    hs = hg.shape[0]
    hw = q.shape[1]
    steps = len(scan_windows(ep))
    fu = wg.shape[2]
    gr = gb * cap
    vm = pltpu.VMEM
    dma = pltpu.SemaphoreType.DMA
    scratch = [
        vm(wm.shape, BF),
        vm(wg.shape[1:], BF),
        vm(wu.shape[1:], BF),
        vm(wd.shape[1:], BF),
        vm((ep, cap, width), BF),
        vm((tp, ep, cap, width), BF),
        vm((gr, fu), BF),
        vm((groups, ny, gr, width), BF),
        vm((groups, ny, gr, width), BF),
        vm((2, ny, gr, width), F32),
        vm((groups, ny, gr, width), BF),
        vm((groups, ny, gr, width), BF),
        vm((ep, cap, width), BF),
        vm((ep, cap, width), BF),
        vm((TOP_K, rows, ep * cap), BF),
        vm((steps, heads, hs + 16, hs), BF),
        vm((steps, heads, hs + 16, hs), BF),
        vm((heads, hs + 16, hs), F32),
        vm((rows, hw), F32),
        vm((rows, hw), BF),
        vm((tp, rows, hw), BF),
        dma((4,)),
        dma((ep,)),
        dma((ep,)),
        dma((groups, ny)),
        dma((groups, ny)),
        dma((groups, ny)),
        dma((groups, ny)),
        dma((groups, ny)),
        dma((groups, ny)),
        dma((groups, ny)),
        dma((groups, ny)),
        dma((ep,)),
        dma((ep,)),
        dma((steps,)),
        dma((steps,)),
        dma((ny,)),
        dma((ny,)),
        dma((ny,)),
        dma((ny,)),
    ]
    out = jax.ShapeDtypeStruct((rows, width), BF)
    in_vm = pl.BlockSpec(memory_space=pltpu.VMEM)
    in_any = pl.BlockSpec(memory_space=pl.ANY)
    made = pl.pallas_call(
        functools.partial(kernel, (ep, tp, cap, groups)),
        out_shape=(out, out),
        in_specs=[in_vm] * 11 + [in_any] * 4,
        out_specs=(in_vm, in_vm),
        scratch_shapes=scratch,
        compiler_params=pltpu.CompilerParams(
            collective_id=0, has_side_effects=True, vmem_limit_bytes=60 * 1024 * 1024
        ),
    )(q, fi, v, og, ds.T, ff[None, :], hg[None, :], x, mg[None, :], rt.T, rw.T, wm, wg, wu, wd)
    return pl.pallas_call(
        emit, out_shape=(out, out), in_specs=[in_vm] * 2, out_specs=(in_vm, in_vm), name="emit"
    )(*made)


def solution(mesh):
    placed = (
        P("ep", "tp"),
        P("ep", "tp"),
        P("ep", "tp"),
        P("ep", "tp"),
        P("ep", "tp"),
        P("tp"),
        P(),
        P(None, "tp"),
        P("ep", None),
        P(),
        P("ep", None),
        P("ep", None),
        P("ep", None, "tp"),
        P("ep", None, "tp"),
        P("ep", "tp", None),
    )
    return jax.shard_map(
        functools.partial(body, mesh.shape["ep"], mesh.shape["tp"]),
        mesh=mesh,
        in_specs=placed,
        out_specs=(P("ep", "tp"), P("ep", "tp")),
        check_vma=False,
    )
```

profile of v0, /device:TPU:0, one launch (start us, length us, event | category | flops | bytes accessed | tf_op | source)
XLA Modules:
  0.0 67.0 jit_solution(4461423724737441598)
XLA Ops:
  0.6 64.5 %shard_map.158 = (bf16[256,512]{1,0:T(8,128)(2,1)}, bf16[256,512]{1,0:T(8,128)(2,1)}) custom-call(bf16[256,512]{1,0:T(8,128)(2,1)} %q_ref.1, bf16[256,512]{1,0:T(8,128)(2,1)} %fi_ref.1, bf16[256,512]{1,0:T(8,128)(2,1)} %v_ref.1, bf16[256,512]{1,0:T(8,128)(2,1)} %og_ref.1, f32[4,256]{1,0:T(4,128)} %bitcast.7, f32[1,512]{1,0:T(1,128)} %bitcast.8, ...), custom_call_target="tpu_custom_call" | custom-call | tf_op jit(solution)/shard_map/pallas_call | solution.py:497
  65.1 1.8 %emit.1 = (bf16[256,512]{1,0:T(8,128)(2,1)}, bf16[256,512]{1,0:T(8,128)(2,1)}) custom-call(bf16[256,512]{1,0:T(8,128)(2,1)} %get-tuple-element.4.a_ref, bf16[256,512]{1,0:T(8,128)(2,1)} %get-tuple-element.5.b_ref), custom_call_target="tpu_custom_call" | custom-call | tf_op jit(solution)/shard_map/emit/pallas_call | solution.py:507
where the time goes:
time: 67.4 us; the launch traced here: 67 us
  Pallas kernels  66.3 us (98%)
    pallas_call x1, Pallas kernels, body(): pl.pallas_call(functools.partial(kernel, (ep, tp, cap, groups)), out_shap...  64.5 us
    pallas_call x1, Pallas kernels, body(): pl.pallas_call(emit, out_shape=(out, out), in_specs=[in_vm] * 2, out_spec...  1.84 us

commit v1 on v0

v1 whole, which is shorter than its diff:
```python
import functools

import jax
import jax.numpy as jnp
from jax import lax
from jax.experimental import pallas as pl
from jax.experimental.pallas import tpu as pltpu
from jax.sharding import PartitionSpec as P

TOP_K = 2
EPS = 1e-06
MESH = pl.DeviceIdType.MESH
BF = jnp.bfloat16
F32 = jnp.float32
HIGH = lax.Precision.HIGHEST
NS = jax.named_scope


def mm(a, b, dims=((1,), (0,)), precision=None):
    return lax.dot_general(
        a, b, (dims, ((), ())), preferred_element_type=F32, precision=precision
    )


def kernel(
    cfg,
    q_hbm,
    fi_hbm,
    v_hbm,
    og_hbm,
    ds_hbm,
    ff_hbm,
    hg_hbm,
    x_hbm,
    mg_hbm,
    rt_hbm,
    rw_hbm,
    wm_hbm,
    wg_hbm,
    wu_hbm,
    wd_hbm,
    mixed_hbm,
    moe_hbm,
    q_ref,
    fi_ref,
    v_ref,
    og_ref,
    ds_ref,
    ff_ref,
    hg_ref,
    x_ref,
    mg_ref,
    rt_ref,
    rw_ref,
    mixed_ref,
    moe_ref,
    wm,
    wg,
    wu,
    wd,
    dispn,
    dispf,
    xs,
    hid,
    snd_p,
    rs_p,
    own,
    snd_y,
    rs_y,
    fin,
    ret,
    wpn,
    wpf,
    kx_s,
    kx_r,
    kc_s,
    kc_r,
    pair,
    carry,
    intra,
    qdec,
    ho,
    in_sem,
    out_sem,
    w_sem,
    a_ss,
    a_rs,
    gy_ss,
    gy_rs,
    gp_ss,
    gp_rs,
    rp_ss,
    rp_rs,
    ry_ss,
    ry_rs,
    b_ss,
    b_rs,
    kx_ss,
    kx_rs,
    kc_ss,
    kc_rs,
    hy_ss,
    hy_rs,
    hp_ss,
    hp_rs,
):
    ep, tp, cap, near = cfg
    far = ep - near
    ny = tp // 2
    me = lax.axis_index("ep")
    t = lax.axis_index("tp")
    y = t // 2
    c = t % 2
    mate = y * 2 + (1 - c)
    rows, dim = x_ref.shape
    width = dim // tp
    slots = ep * cap
    hidden_units = wg.shape[1]
    heads = ds_ref.shape[0]
    hs = hg_ref.shape[1]
    hw = q_ref.shape[1]
    hpn = ho.shape[2]
    cw = hw // hpn
    bits = ep.bit_length() - 1
    me_bits = [lax.rem(lax.div(me, 2**k), 2) for k in range(bits)]
    zi = lax.div(me, 2)
    nz = ep // 2
    xb = me_bits[0]

    def ring(a, n):
        return lax.rem(a + n, n)

    def up_y(dy):
        return ring(y + dy, ny)

    def dn_y(dy):
        return ring(y - dy, ny)

    def peer(mask):
        out = 0
        for k in range(bits):
            out = out + (1 - me_bits[k] if (mask >> k) & 1 else me_bits[k]) * 2**k
        return out

    def peer_dyn(mask):
        out = 0
        for k in range(bits):
            m = lax.rem(lax.div(mask, 2**k), 2)
            out = out + lax.rem(me_bits[k] + m, 2) * 2**k
        return out

    def rc(src, dst, ss, rs, e, j):
        return pltpu.make_async_remote_copy(
            src_ref=src, dst_ref=dst, send_sem=ss, recv_sem=rs, device_id=(e, j), device_id_type=MESH
        )

    loads = [
        pltpu.make_async_copy(wg_hbm.at[0], wg, w_sem.at[0]),
        pltpu.make_async_copy(wu_hbm.at[0], wu, w_sem.at[1]),
        pltpu.make_async_copy(wd_hbm.at[0], wd, w_sem.at[2]),
        pltpu.make_async_copy(wm_hbm, wm, w_sem.at[3]),
    ]
    small = {}
    pairs = (
        ("rt", rt_hbm, rt_ref),
        ("x", x_hbm, x_ref),
        ("mg", mg_hbm, mg_ref),
        ("fi", fi_hbm, fi_ref),
        ("ff", ff_hbm, ff_ref),
        ("ds", ds_hbm, ds_ref),
        ("v", v_hbm, v_ref),
        ("q", q_hbm, q_ref),
        ("rw", rw_hbm, rw_ref),
        ("og", og_hbm, og_ref),
        ("hg", hg_hbm, hg_ref),
    )
    for i, (name, src, dst) in enumerate(pairs):
        small[name] = pltpu.make_async_copy(src, dst, in_sem.at[i])
    for name in ("rt", "x", "mg"):
        small[name].start()
    barrier = pltpu.get_barrier_semaphore()
    for d in range(1, ep):
        pl.semaphore_signal(barrier, inc=1, device_id=(ring(me + d, ep), t), device_id_type=MESH)
    for dy in range(1, ny):
        pl.semaphore_signal(barrier, inc=1, device_id=(me, up_y(dy) * 2 + c), device_id_type=MESH)
    pl.semaphore_signal(barrier, inc=1, device_id=(me, mate), device_id_type=MESH)

    gn, gf = near // 2, far // 2
    inner = lax.rem(me_bits[1] + me_bits[2], 2) if bits > 2 else 0
    groups = [
        (0, gn, 0, True),
        (near + gf * (1 - inner), gf, gn * cap, False),
        (gn, gn, (gn + gf) * cap, True),
        (near + gf * inner, gf, (2 * gn + gf) * cap, False),
    ]

    def a2a(p):
        if p < near:
            return rc(dispn.at[:, p], xs.at[:, c, p], a_ss.at[p], a_rs.at[p], peer(p), t)
        return rc(dispf.at[p - near], xs.at[y, c, p], a_ss.at[p], a_rs.at[p], peer(p), t)

    def a2a_in(p, is_near):
        r = xs.at[:, c, p] if is_near else xs.at[y, c, p]
        return rc(r, r, a_ss.at[p], a_rs.at[p], me, mate)

    def near_p(p):
        r = xs.at[:, c, p]
        return rc(r, r, gp_ss.at[0, p], gp_rs.at[0, p], me, mate)

    def near_p_in(p):
        r = xs.at[:, 1 - c, p]
        return rc(r, r, gp_ss.at[0, p], gp_rs.at[0, p], me, mate)

    def gat_y(p, dy):
        r = xs.at[y, c, p]
        return rc(r, r, gy_ss.at[dy, p], gy_rs.at[dy, p], me, up_y(dy) * 2 + c)

    def gat_y_in(p, dy):
        r = xs.at[dn_y(dy), c, p]
        return rc(r, r, gy_ss.at[dy, p], gy_rs.at[dy, p], me, mate)

    def gat_p(p, dy):
        r = xs.at[dn_y(dy), c, p]
        return rc(r, r, gp_ss.at[dy, p], gp_rs.at[dy, p], me, mate)

    def gat_p_in(p, dy):
        r = xs.at[dn_y(dy), 1 - c, p]
        return rc(r, r, gp_ss.at[dy, p], gp_rs.at[dy, p], me, mate)

    def take_near(p):
        with NS(f"take_near{p}"):
            if p:
                a2a_in(p, True).wait_recv()
            near_p(p).start()

    def take_far(g, i):
        with NS(f"take_far{g}"):
            p = groups[g][0] + i
            a2a_in(p, False).wait_recv()
            for dy in range(1, ny):
                gat_y(p, dy).start()
            gat_p(p, 0).start()

    def relay_far(g, i):
        with NS(f"relay_far{g}"):
            p = groups[g][0] + i
            for dy in range(1, ny):
                gat_y_in(p, dy).wait_recv()
                gat_p(p, dy).start()

    def arrived(g):
        with NS(f"arrived{g}"):
            base, n, _, is_near = groups[g]
            for i in range(n):
                if is_near:
                    near_p_in(base + i).wait_recv()
                else:
                    for dy in range(ny):
                        gat_p_in(base + i, dy).wait_recv()

    with NS("rt_wait"):
        small["rt"].wait()
    with NS("route"):
        i_r = lax.broadcasted_iota(jnp.int32, (rows, rows), 0)
        i_c = lax.broadcasted_iota(jnp.int32, (rows, rows), 1)
        hr = max(8, ep)
        p_row = lax.broadcasted_iota(jnp.int32, (hr, rows), 0)
        pos, hot = [], []
        for k in range(TOP_K):
            r = jnp.bitwise_xor(rt_ref[k : k + 1, :], me)
            pos.append(r)
            hot.append((p_row == r).astype(F32))
        before = mm(sum(hot).astype(BF), (i_r < i_c).astype(F32).astype(BF))
        slot = []
        for k in range(TOP_K):
            rank = jnp.sum(before * hot[k], axis=0, keepdims=True).astype(jnp.int32)
            slot.append(pos[k] * cap + rank)
        s_row = lax.broadcasted_iota(jnp.int32, (slots, rows), 0)
        hits = [s_row == slot[k] for k in range(TOP_K)]
        pick = jnp.where(hits[0], 1.0, jnp.where(hits[1], 1.0, 0.0)).astype(BF)
    with NS("x_wait"):
        small["x"].wait()
        small["mg"].wait()
        for name in ("fi", "ff", "ds", "v", "q", "rw", "og", "hg"):
            small[name].start()
    with NS("norm"):
        xf = x_ref[...].astype(F32)
        inv = lax.rsqrt(jnp.mean(xf * xf, axis=1, keepdims=True) + EPS)

        def normed(yy):
            cols = pl.ds(pl.multiple_of((yy * 2 + c) * width, width), width)
            return (x_ref[:, cols].astype(F32) * inv * mg_ref[:, cols]).astype(BF)

    nr = near * cap
    with NS("disp_near"):
        for yy in range(ny):
            out = mm(pick[0:nr], normed(yy)).astype(BF).reshape(near, cap, width)
            dispn[yy] = out
            xs[yy, c, 0] = out[0]
    with NS("bar"):
        pl.semaphore_wait(barrier, ep - 1 + ny)
    for p in range(1, gn):
        a2a(p).start()
    with NS("disp_far"):
        dispf[...] = mm(pick[nr:], normed(y)).astype(BF).reshape(far, cap, width)
    for p in list(range(near, ep)) + list(range(gn, near)):
        a2a(p).start()
    take_near(0)

    causal = i_r >= i_c
    tri = causal.astype(F32)

    def mix_all_decay():
        fl = ff_ref[...]
        fx = fi_ref[...].astype(F32)
        forget = fl + (1.0 - fl) * jax.nn.sigmoid(fx)
        return mm(tri, jnp.log(forget), precision=HIGH)

    def state_x(h):
        return rc(kx_s.at[h], kx_r.at[h], kx_ss.at[h], kx_rs.at[h], peer(1), t)

    def mix_head(h, run, s_col, s_row):
        hc = slice(h * hs, (h + 1) * hs)
        lr = run[:, hc]
        sc = s_col[:, h : h + 1]
        sr = s_row[h : h + 1, :]
        key = (1.0 - ff_ref[:, hc]) * jax.nn.sigmoid(-fi_ref[:, hc].astype(F32))
        v = v_ref[:, hc]
        l_end = lr[rows - 1 : rows, :]
        s_end = sc[rows - 1 : rows, :]
        kd = (key * jnp.exp(l_end - lr + (s_end - sc))).astype(BF)
        kx_s[h, 0:hs, :] = mm(v, kd, ((0,), (0,))).astype(BF)
        kx_s[h, hs : hs + 16, :] = jnp.broadcast_to(jnp.exp(l_end + s_end), (16, hs)).astype(BF)
        state_x(h).start()
        q = q_ref[:, hc].astype(F32) * jnp.exp(lr)
        scores = mm(q.astype(BF), (key * jnp.exp(-lr)).astype(BF), ((1,), (1,)))
        scores = jnp.where(causal, scores * jnp.exp(jnp.minimum(sc - sr, 0.0)), 0.0)
        intra[:, hc] = mm(scores.astype(BF), v)
        qdec[:, hc] = (q * jnp.exp(sc)).astype(BF)

    with NS("mix_wait"):
        for name in ("fi", "ff", "ds", "v", "q", "rw", "og", "hg"):
            small[name].wait()
        for load in loads:
            load.start()
    with NS("decay"):
        run = mix_all_decay()
        s_col = mm(tri, ds_ref[...], ((1,), (1,)), HIGH)
        s_rows = mm(ds_ref[...], tri, ((1,), (1,)), HIGH)
    for h in range(heads):
        with NS(f"head{h}"):
            mix_head(h, run, s_col, s_rows)
    with NS("weights"):
        wp = jnp.where(hits[0], rw_ref[0:1, :], jnp.where(hits[1], rw_ref[1:2, :], 0.0))
        wpn[...] = wp[0:nr].T.astype(BF)
        wpf[...] = wp[nr:].T.astype(BF)

    def chain_copy(h):
        return rc(kc_s.at[h], kc_r.at[h], kc_ss.at[h], kc_rs.at[h], ring(me + 2, ep), t)

    def pair_states():
        for h in range(heads):
            with NS("state_wait"):
                state_x(h).wait_recv()
            mine = kx_s[h].astype(F32)
            other = kx_r[h].astype(F32)
            one = jnp.where(xb == 0, mine, other)
            two = jnp.where(xb == 0, other, mine)
            a_two = two[hs : hs + 1]
            both = a_two * one[0:hs] + two[0:hs]
            pair[h, 0:hs, :] = both
            pair[h, hs : hs + 8, :] = a_two * one[hs : hs + 8]

            @pl.when(zi == 0)
            def _():
                carry[h] = jnp.where(xb == 0, 0.0, other[0:hs]).astype(BF)
                kc_s[h] = both.astype(BF)
                chain_copy(h).start()

    def chain(s):
        @pl.when(zi == s)
        def _():
            for h in range(heads):
                chain_copy(h).wait_recv()
                p = kc_r[h].astype(F32)
                if s + 1 < nz:
                    kc_s[h] = (pair[h, hs : hs + 1, :] * p + pair[h, 0:hs, :]).astype(BF)
                    chain_copy(h).start()
                other = kx_r[h].astype(F32)
                carry[h] = jnp.where(xb == 0, p, other[hs : hs + 1] * p + other[0:hs]).astype(BF)

    def ho_y(p, dy):
        r = ho.at[y, c, p]
        return rc(r, r, hy_ss.at[p, dy], hy_rs.at[p, dy], me, up_y(dy) * 2 + c)

    def ho_y_in(p, dy):
        r = ho.at[dn_y(dy), c, p]
        return rc(r, r, hy_ss.at[p, dy], hy_rs.at[p, dy], me, mate)

    def ho_p(p, dy):
        r = ho.at[dn_y(dy), c, p]
        return rc(r, r, hp_ss.at[p, dy], hp_rs.at[p, dy], me, mate)

    def ho_p_in(p, dy):
        r = ho.at[dn_y(dy), 1 - c, p]
        return rc(r, r, hp_ss.at[p, dy], hp_rs.at[p, dy], me, mate)

    def mix_close():
        for p in range(hpn):
            with NS("close"):
                for i in range(cw // hs):
                    h = p * (cw // hs) + i
                    hc = slice(h * hs, (h + 1) * hs)
                    o = intra[:, hc] + mm(qdec[:, hc], carry[h], ((1,), (1,)))
                    iv = lax.rsqrt(jnp.mean(o * o, axis=1, keepdims=True) + EPS)
                    g = og_ref[:, hc].astype(F32)
                    ho[y, c, p, :, i * hs : (i + 1) * hs] = (
                        o * iv * hg_ref[...] * (g * jax.nn.sigmoid(g))
                    ).astype(BF)
                for dy in range(1, ny):
                    ho_y(p, dy).start()
                ho_p(p, 0).start()

    def ho_relay():
        with NS("ho_relay"):
            for p in range(hpn):
                for dy in range(1, ny):
                    ho_y_in(p, dy).wait_recv()
                    ho_p(p, dy).start()

    def project():
        with NS("ho_wait"):
            for p in range(hpn):
                for dy in range(ny):
                    ho_p_in(p, dy).wait_recv()
        with NS("proj"):
            acc = jnp.zeros(mixed_ref.shape, F32)
            for j in range(tp):
                for p in range(hpn):
                    k0 = j * hw + p * cw
                    acc += mm(ho[j // 2, j % 2, p], wm[k0 : k0 + cw, :])
            mixed_ref[...] = acc.astype(BF)
            pltpu.make_async_copy(mixed_ref, mixed_hbm, out_sem.at[0]).start()

    ft = min(256, hidden_units)

    tiles = hidden_units // ft

    def first(g, between=None):
        if between is None:
            first_part(g, 0, tiles)
        else:
            first_part(g, 0, tiles // 2)
            between()
            first_part(g, tiles // 2, tiles)

    def first_part(g, lo, hi):
        with NS(f"first{g}"):
            base, n, _, is_near = groups[g]
            gr = n * cap

            def tile(k, _):
                fc = pl.ds(pl.multiple_of(k * ft, ft), ft)
                gate = jnp.zeros((gr, ft), F32)
                up = jnp.zeros((gr, ft), F32)
                for j in range(tp):
                    a = xs[j // 2, j % 2, pl.ds(base, n)].reshape(gr, width)
                    gate += mm(a, wg[j * width : (j + 1) * width, fc])
                    up += mm(a, wu[j * width : (j + 1) * width, fc])
                hid[0:gr, fc] = (gate * jax.nn.sigmoid(gate) * up).astype(BF)
                return 0

            lax.fori_loop(lo, hi, tile, 0)

    def red_p(g, dy):
        _, n, r0, _ = groups[g]
        rs = pl.ds(r0, n * cap)
        return rc(snd_p.at[dy, rs], rs_p.at[dy, rs], rp_ss.at[g, dy], rp_rs.at[g, dy], me, mate)

    def red_y(g, i, dy):
        r0 = groups[g][2] + i * cap
        b = r0 // cap
        rs = pl.ds(r0, cap)
        return rc(
            snd_y.at[dy, rs], rs_y.at[dy, rs], ry_ss.at[b, dy], ry_rs.at[b, dy], me, up_y(dy) * 2 + c
        )

    order = list(range(1, ny)) + [0]

    def second(g):
        _, n, r0, _ = groups[g]
        gr = n * cap

        def down(dy, core):
            col = up_y(dy) * 2 + core
            return mm(hid[0:gr], wd[:, pl.ds(pl.multiple_of(col * width, width), width)])

        with NS(f"second{g}"):
            for dy in order:
                snd_p[dy, r0 : r0 + gr] = down(dy, 1 - c).astype(BF)
                red_p(g, dy).start()
            for dy in order:
                own[dy, r0 : r0 + gr] = down(dy, c)

    def reduce_p(g):
        _, n, r0, _ = groups[g]
        with NS(f"reduce_p{g}"):
            for dy in order:
                red_p(g, dy).wait_recv()
                for i in range(n):
                    rr = slice(r0 + i * cap, r0 + (i + 1) * cap)
                    total = own[dy, rr] + rs_p[dy, rr].astype(F32)
                    if dy:
                        snd_y[dy, rr] = total.astype(BF)
                        red_y(g, i, dy).start()
                    else:
                        own[0, rr] = total

    def back(g, i):
        base, _, r0, is_near = groups[g]
        b = r0 // cap + i
        p = base + i
        dest = peer(p) if is_near else peer_dyn(p)
        return rc(fin.at[b], ret.at[p], b_ss.at[b], b_rs.at[p], dest, t)

    def give_back(g):
        _, n, r0, _ = groups[g]
        with NS(f"give_back{g}"):
            for i in range(n):
                rr = slice(r0 + i * cap, r0 + (i + 1) * cap)
                total = own[0, rr]
                for dy in range(1, ny):
                    red_y(g, i, dy).wait_recv()
                    total += rs_y[dy, rr].astype(F32)
                if g == 0 and i == 0:
                    ret[0] = total.astype(BF)
                else:
                    fin[r0 // cap + i] = total.astype(BF)
                    back(g, i).start()

    def back_in(p):
        return rc(fin.at[p], ret.at[p], b_ss.at[p], b_rs.at[p], me, mate)

    def far_taken(g):
        for i in range(gf):
            take_far(g, i)

    def far_relayed(g):
        for i in range(gf):
            relay_far(g, i)

    def chain_at(lo, hi):
        with NS(f"chain{lo}"):
            for s in range(lo, min(hi, nz)):
                chain(s)

    for p in range(1, gn):
        take_near(p)
    with NS("loads"):
        for load in loads[:3]:
            load.wait()
    arrived(0)
    first(0, lambda: take_far(1, 0))
    for i in range(1, gf):
        take_far(1, i)
    second(0)
    with NS("pair_states"):
        pair_states()
    far_relayed(1)
    reduce_p(0)
    arrived(1)
    first(1)
    for p in range(gn, near):
        take_near(p)
    far_taken(3)
    second(1)
    chain_at(1, 2)
    give_back(0)
    reduce_p(1)
    arrived(2)
    first(2)
    far_relayed(3)
    second(2)
    chain_at(2, 3)
    reduce_p(2)
    arrived(3)
    first(3)
    give_back(1)
    second(3)
    chain_at(3, nz)
    reduce_p(3)
    mix_close()
    give_back(2)
    give_back(3)
    ho_relay()
    loads[3].wait()
    project()
    with NS("near_back"):
        for p in range(1, near):
            back_in(p).wait_recv()
    with NS("comb_near"):
        res = mm(wpn[...], ret[0:near].reshape(nr, width))
    with NS("far_back"):
        for p in range(near, ep):
            back_in(p).wait_recv()
    with NS("comb_far"):
        res += mm(wpf[...], ret[near:].reshape(slots - nr, width))
        moe_ref[...] = res.astype(BF)
        pltpu.make_async_copy(moe_ref, moe_hbm, out_sem.at[1]).start()

    with NS("drain"):
        for p in range(1, ep):
            a2a(p).wait_send()
        for g, (base, n, r0, is_near) in enumerate(groups):
            for i in range(n):
                if g or i:
                    back(g, i).wait_send()
                for dy in range(1, ny):
                    red_y(g, i, dy).wait_send()
                if is_near:
                    near_p(base + i).wait_send()
                else:
                    for dy in range(ny):
                        gat_p(base + i, dy).wait_send()
                        if dy:
                            gat_y(base + i, dy).wait_send()
            for dy in range(ny):
                red_p(g, dy).wait_send()
        for h in range(heads):
            state_x(h).wait_send()
            pl.when(zi + 1 < nz)(lambda h=h: chain_copy(h).wait_send())
        for p in range(hpn):
            for dy in range(ny):
                ho_p(p, dy).wait_send()
                if dy:
                    ho_y(p, dy).wait_send()
        pltpu.make_async_copy(mixed_ref, mixed_hbm, out_sem.at[0]).wait()
        pltpu.make_async_copy(moe_ref, moe_hbm, out_sem.at[1]).wait()


def emit(a_ref, b_ref, a_out, b_out, held, sem):
    copies = [
        (
            pltpu.make_async_copy(src, held.at[i], sem.at[i, 0]),
            pltpu.make_async_copy(held.at[i], dst, sem.at[i, 1]),
        )
        for i, (src, dst) in enumerate(((a_ref, a_out), (b_ref, b_out)))
    ]
    for take, _ in copies:
        take.start()
    for take, give in copies:
        take.wait()
        give.start()
    for _, give in copies:
        give.wait()


def body(ep, tp, *args):
    (q, fi, v, og, ds, ff, hg, wm, x, mg, rt, rw, wg, wu, wd) = args
    rows, dim = x.shape
    capacity = 5 * rows * TOP_K // (4 * ep)
    cap = -(-capacity // 16) * 16
    near = min(4, ep // 2)
    ny = tp // 2
    width = dim // tp
    heads = ds.shape[1]
    hs = hg.shape[0]
    hw = q.shape[1]
    hpn = max(1, heads // 2)
    fu = wg.shape[2]
    slots = ep * cap
    gmax = max(near // 2, (ep - near) // 2) * cap
    vm = pltpu.VMEM
    dma = pltpu.SemaphoreType.DMA
    operands = (q, fi, v, og, ds.T, ff[None, :], hg[None, :], x, mg[None, :], rt.T, rw.T)
    scratch = [vm(a.shape, a.dtype) for a in operands] + [
        vm((rows, width), BF),
        vm((rows, width), BF),
        vm(wm.shape, BF),
        vm(wg.shape[1:], BF),
        vm(wu.shape[1:], BF),
        vm(wd.shape[1:], BF),
        vm((ny, near, cap, width), BF),
        vm((ep - near, cap, width), BF),
        vm((ny, 2, ep, cap, width), BF),
        vm((gmax, fu), BF),
        vm((ny, slots, width), BF),
        vm((ny, slots, width), BF),
        vm((ny, slots, width), F32),
        vm((ny, slots, width), BF),
        vm((ny, slots, width), BF),
        vm((ep, cap, width), BF),
        vm((ep, cap, width), BF),
        vm((rows, near * cap), BF),
        vm((rows, slots - near * cap), BF),
        vm((heads, hs + 16, hs), BF),
        vm((heads, hs + 16, hs), BF),
        vm((heads, hs, hs), BF),
        vm((heads, hs, hs), BF),
        vm((heads, hs + 8, hs), F32),
        vm((heads, hs, hs), BF),
        vm((rows, hw), F32),
        vm((rows, hw), BF),
        vm((ny, 2, hpn, rows, hw // hpn), BF),
        dma((len(operands),)),
        dma((2,)),
        dma((4,)),
        dma((ep,)),
        dma((ep,)),
        dma((ny, ep)),
        dma((ny, ep)),
        dma((ny, ep)),
        dma((ny, ep)),
        dma((4, ny)),
        dma((4, ny)),
        dma((ep, ny)),
        dma((ep, ny)),
        dma((ep,)),
        dma((ep,)),
        dma((heads,)),
        dma((heads,)),
        dma((heads,)),
        dma((heads,)),
        dma((hpn, ny)),
        dma((hpn, ny)),
        dma((hpn, ny)),
        dma((hpn, ny)),
    ]
    out = jax.ShapeDtypeStruct((rows, width), BF)
    in_any = pl.BlockSpec(memory_space=pl.ANY)
    made = pl.pallas_call(
        functools.partial(kernel, (ep, tp, cap, near)),
        out_shape=(out, out),
        in_specs=[in_any] * 15,
        out_specs=(in_any, in_any),
        scratch_shapes=scratch,
        compiler_params=pltpu.CompilerParams(
            collective_id=0, has_side_effects=True, vmem_limit_bytes=60 * 1024 * 1024
        ),
    )(*operands, wm, wg, wu, wd)
    return pl.pallas_call(
        emit,
        out_shape=(out, out),
        in_specs=[in_any] * 2,
        out_specs=(in_any, in_any),
        scratch_shapes=[vm((2, rows, width), BF), dma((2, 2))],
        name="emit",
    )(*made)


def solution(mesh):
    placed = (
        P("ep", "tp"),
        P("ep", "tp"),
        P("ep", "tp"),
        P("ep", "tp"),
        P("ep", "tp"),
        P("tp"),
        P(),
        P(None, "tp"),
        P("ep", None),
        P(),
        P("ep", None),
        P("ep", None),
        P("ep", None, "tp"),
        P("ep", None, "tp"),
        P("ep", "tp", None),
    )
    return jax.shard_map(
        functools.partial(body, mesh.shape["ep"], mesh.shape["tp"]),
        mesh=mesh,
        in_specs=placed,
        out_specs=(P("ep", "tp"), P("ep", "tp")),
        check_vma=False,
    )
```

time: 67.4 us -> 53.7 us (0.80)
  Pallas kernels: 66.3 us -> 52.5 us
    pallas_call x2, Pallas kernels: 66.3 us -> 52.5 us  [the longest x1 50.7 us: body(): pl.pallas_call(functools.partial(kernel, (ep, tp, cap, near)), out_shape=...]
where the time goes in v1:
time: 53.7 us; the launch traced here: 53.1 us
  Pallas kernels  52.5 us (98%)
  between operations  0.64 us (1%)
    pallas_call x1, Pallas kernels, body(): pl.pallas_call(functools.partial(kernel, (ep, tp, cap, near)), out_shape=...  50.7 us
    pallas_call x1, Pallas kernels, body(): pl.pallas_call(emit, out_shape=(out, out), in_specs=[in_any] * 2, out_spe...  1.77 us

profile of v1, /device:TPU:0, one launch (start us, length us, event | category | flops | bytes accessed | tf_op | source)
XLA Modules:
  0.0 53.1 jit_solution(4123645183176639364)
XLA Ops:
  0.6 50.7 %shard_map.158 = (bf16[256,512]{1,0:T(8,128)(2,1)}, bf16[256,512]{1,0:T(8,128)(2,1)}) custom-call(bf16[256,512]{1,0:T(8,128)(2,1)} %q_hbm.1, bf16[256,512]{1,0:T(8,128)(2,1)} %fi_hbm.1, bf16[256,512]{1,0:T(8,128)(2,1)} %v_hbm.1, bf16[256,512]{1,0:T(8,128)(2,1)} %og_hbm.1, f32[4,256]{1,0:T(4,128)} %bitcast.7, f32[1,512]{1,0:T(1,128)} %bitcast.8, ...), custom_call_target="tpu_custom_call" | custom-call | tf_op jit(solution)/shard_map/pallas_call | solution.py:731
  51.3 1.8 %emit.1 = (bf16[256,512]{1,0:T(8,128)(2,1)}, bf16[256,512]{1,0:T(8,128)(2,1)}) custom-call(bf16[256,512]{1,0:T(8,128)(2,1)} %get-tuple-element.4.a_ref, bf16[256,512]{1,0:T(8,128)(2,1)} %get-tuple-element.5.b_ref), custom_call_target="tpu_custom_call" | custom-call | tf_op jit(solution)/shard_map/emit/pallas_call | solution.py:741

commit v2 on v1

--- a/solution.py
+++ b/solution.py
@@ -83,25 +83,18 @@
     in_sem,
     out_sem,
     w_sem,
-    a_ss,
+    sends,
+    n_rs,
     a_rs,
-    gy_ss,
+    gn_rs,
     gy_rs,
-    gp_ss,
     gp_rs,
-    rp_ss,
     rp_rs,
-    ry_ss,
     ry_rs,
-    b_ss,
     b_rs,
-    kx_ss,
     kx_rs,
-    kc_ss,
     kc_rs,
-    hy_ss,
     hy_rs,
-    hp_ss,
     hp_rs,
 ):
     ep, tp, cap, near = cfg
@@ -187,76 +180,92 @@
 
     gn, gf = near // 2, far // 2
     inner = lax.rem(me_bits[1] + me_bits[2], 2) if bits > 2 else 0
+    early = [near + gf * (1 - inner) + i for i in range(gf)]
+    late = [near + gf * inner + i for i in range(gf)]
+    hf = gf // 2
     groups = [
-        (0, gn, 0, True),
-        (near + gf * (1 - inner), gf, gn * cap, False),
-        (gn, gn, (gn + gf) * cap, True),
-        (near + gf * inner, gf, (2 * gn + gf) * cap, False),
+        [(p, True) for p in range(gn)],
+        [(p, False) for p in early],
+        [(p, False) for p in late[:hf]] + [(p, True) for p in range(gn, near)],
+        [(p, False) for p in late[hf:]],
     ]
-
-    def a2a(p):
-        if p < near:
-            return rc(dispn.at[:, p], xs.at[:, c, p], a_ss.at[p], a_rs.at[p], peer(p), t)
-        return rc(dispf.at[p - near], xs.at[y, c, p], a_ss.at[p], a_rs.at[p], peer(p), t)
-
-    def a2a_in(p, is_near):
-        r = xs.at[:, c, p] if is_near else xs.at[y, c, p]
-        return rc(r, r, a_ss.at[p], a_rs.at[p], me, mate)
-
-    def near_p(p):
-        r = xs.at[:, c, p]
-        return rc(r, r, gp_ss.at[0, p], gp_rs.at[0, p], me, mate)
-
-    def near_p_in(p):
-        r = xs.at[:, 1 - c, p]
-        return rc(r, r, gp_ss.at[0, p], gp_rs.at[0, p], me, mate)
+    first_of = [sum(len(g) for g in groups[:i]) for i in range(len(groups))]
+
+    kinds = ("near", "far", "gn", "gy", "gp", "rp", "ry", "back", "kx", "kc", "hy", "hp")
+    sem = {kind: sends.at[i] for i, kind in enumerate(kinds)}
+
+    def near_a2a(p, yy):
+        return rc(dispn.at[yy, p], xs.at[yy, c, p], sem["near"], n_rs.at[p, yy], peer(p), t)
+
+    def near_a2a_in(p, yy):
+        r = xs.at[yy, c, p]
+        return rc(r, r, sem["near"], n_rs.at[p, yy], me, mate)
+
+    def far_a2a(p):
+        return rc(dispf.at[p - near], xs.at[y, c, p], sem["far"], a_rs.at[p - near], peer_dyn(p), t)
+
+    def far_a2a_in(p):
+        r = xs.at[y, c, p]
+        return rc(r, r, sem["far"], a_rs.at[p - near], me, mate)
+
+    def near_p(p, yy):
+        r = xs.at[yy, c, p]
+        return rc(r, r, sem["gn"], gn_rs.at[p, yy], me, mate)
+
+    def near_p_in(p, yy):
+        r = xs.at[yy, 1 - c, p]
+        return rc(r, r, sem["gn"], gn_rs.at[p, yy], me, mate)
 
     def gat_y(p, dy):
         r = xs.at[y, c, p]
-        return rc(r, r, gy_ss.at[dy, p], gy_rs.at[dy, p], me, up_y(dy) * 2 + c)
+        return rc(r, r, sem["gy"], gy_rs.at[dy - 1, p - near], me, up_y(dy) * 2 + c)
 
     def gat_y_in(p, dy):
         r = xs.at[dn_y(dy), c, p]
-        return rc(r, r, gy_ss.at[dy, p], gy_rs.at[dy, p], me, mate)
+        return rc(r, r, sem["gy"], gy_rs.at[dy - 1, p - near], me, mate)
 
     def gat_p(p, dy):
         r = xs.at[dn_y(dy), c, p]
-        return rc(r, r, gp_ss.at[dy, p], gp_rs.at[dy, p], me, mate)
+        return rc(r, r, sem["gp"], gp_rs.at[dy, p - near], me, mate)
 
     def gat_p_in(p, dy):
         r = xs.at[dn_y(dy), 1 - c, p]
-        return rc(r, r, gp_ss.at[dy, p], gp_rs.at[dy, p], me, mate)
+        return rc(r, r, sem["gp"], gp_rs.at[dy, p - near], me, mate)
 
     def take_near(p):
         with NS(f"take_near{p}"):
-            if p:
-                a2a_in(p, True).wait_recv()
-            near_p(p).start()
-
-    def take_far(g, i):
-        with NS(f"take_far{g}"):
-            p = groups[g][0] + i
-            a2a_in(p, False).wait_recv()
-            for dy in range(1, ny):
-                gat_y(p, dy).start()
-            gat_p(p, 0).start()
-
-    def relay_far(g, i):
-        with NS(f"relay_far{g}"):
-            p = groups[g][0] + i
-            for dy in range(1, ny):
-                gat_y_in(p, dy).wait_recv()
-                gat_p(p, dy).start()
+            for yy in range(ny):
+                if p:
+                    near_a2a_in(p, yy).wait_recv()
+                near_p(p, yy).start()
+
+    def far_of(g):
+        return [p for p, is_near in groups[g] if not is_near]
+
+    def take_far(g, lo=0, hi=ep):
+        for p in far_of(g)[lo:hi]:
+            with NS(f"take_far{g}"):
+                far_a2a_in(p).wait_recv()
+                for dy in range(1, ny):
+                    gat_y(p, dy).start()
+                gat_p(p, 0).start()
+
+    def relay_far(g, lo=0, hi=ep):
+        for p in far_of(g)[lo:hi]:
+            with NS(f"relay_far{g}"):
+                for dy in range(1, ny):
+                    gat_y_in(p, dy).wait_recv()
+                    gat_p(p, dy).start()
 
     def arrived(g):
         with NS(f"arrived{g}"):
-            base, n, _, is_near = groups[g]
-            for i in range(n):
+            for p, is_near in groups[g]:
                 if is_near:
-                    near_p_in(base + i).wait_recv()
+                    for yy in range(ny):
+                        near_p_in(p, yy).wait_recv()
                 else:
                     for dy in range(ny):
-                        gat_p_in(base + i, dy).wait_recv()
+                        gat_p_in(p, dy).wait_recv()
 
     with NS("rt_wait"):
         small["rt"].wait()
@@ -299,12 +308,19 @@
             xs[yy, c, 0] = out[0]
     with NS("bar"):
         pl.semaphore_wait(barrier, ep - 1 + ny)
+    def near_send(p):
+        for yy in range(ny):
+            near_a2a(p, yy).start()
+
     for p in range(1, gn):
-        a2a(p).start()
+        near_send(p)
     with NS("disp_far"):
         dispf[...] = mm(pick[nr:], normed(y)).astype(BF).reshape(far, cap, width)
-    for p in list(range(near, ep)) + list(range(gn, near)):
-        a2a(p).start()
+    for i in range(gf):
+        for p in (early[i], late[i]):
+            far_a2a(p).start()
+    for p in range(gn, near - 1):
+        near_send(p)
     take_near(0)
 
     causal = i_r >= i_c
@@ -317,7 +333,7 @@
         return mm(tri, jnp.log(forget), precision=HIGH)
 
     def state_x(h):
-        return rc(kx_s.at[h], kx_r.at[h], kx_ss.at[h], kx_rs.at[h], peer(1), t)
+        return rc(kx_s.at[h], kx_r.at[h], sem["kx"], kx_rs.at[h], peer(1), t)
 
     def mix_head(h, run, s_col, s_row):
         hc = slice(h * hs, (h + 1) * hs)
@@ -356,12 +372,11 @@
         wpf[...] = wp[nr:].T.astype(BF)
 
     def chain_copy(h):
-        return rc(kc_s.at[h], kc_r.at[h], kc_ss.at[h], kc_rs.at[h], ring(me + 2, ep), t)
+        return rc(kc_s.at[h], kc_r.at[h], sem["kc"], kc_rs.at[h], ring(me + 2, ep), t)
 
     def pair_states():
         for h in range(heads):
-            with NS("state_wait"):
-                state_x(h).wait_recv()
+            state_x(h).wait_recv()
             mine = kx_s[h].astype(F32)
             other = kx_r[h].astype(F32)
             one = jnp.where(xb == 0, mine, other)
@@ -391,22 +406,22 @@
 
     def ho_y(p, dy):
         r = ho.at[y, c, p]
-        return rc(r, r, hy_ss.at[p, dy], hy_rs.at[p, dy], me, up_y(dy) * 2 + c)
+        return rc(r, r, sem["hy"], hy_rs.at[p, dy - 1], me, up_y(dy) * 2 + c)
 
     def ho_y_in(p, dy):
         r = ho.at[dn_y(dy), c, p]
-        return rc(r, r, hy_ss.at[p, dy], hy_rs.at[p, dy], me, mate)
+        return rc(r, r, sem["hy"], hy_rs.at[p, dy - 1], me, mate)
 
     def ho_p(p, dy):
         r = ho.at[dn_y(dy), c, p]
-        return rc(r, r, hp_ss.at[p, dy], hp_rs.at[p, dy], me, mate)
+        return rc(r, r, sem["hp"], hp_rs.at[p, dy], me, mate)
 
     def ho_p_in(p, dy):
         r = ho.at[dn_y(dy), 1 - c, p]
-        return rc(r, r, hp_ss.at[p, dy], hp_rs.at[p, dy], me, mate)
-
-    def mix_close():
-        for p in range(hpn):
+        return rc(r, r, sem["hp"], hp_rs.at[p, dy], me, mate)
+
+    def mix_close(lo=0, hi=ep):
+        for p in range(hpn)[lo:hi]:
             with NS("close"):
                 for i in range(cw // hs):
                     h = p * (cw // hs) + i
@@ -456,15 +471,14 @@
 
     def first_part(g, lo, hi):
         with NS(f"first{g}"):
-            base, n, _, is_near = groups[g]
-            gr = n * cap
+            gr = len(groups[g]) * cap
 
             def tile(k, _):
                 fc = pl.ds(pl.multiple_of(k * ft, ft), ft)
                 gate = jnp.zeros((gr, ft), F32)
                 up = jnp.zeros((gr, ft), F32)
                 for j in range(tp):
-                    a = xs[j // 2, j % 2, pl.ds(base, n)].reshape(gr, width)
+                    a = jnp.concatenate([xs[j // 2, j % 2, p] for p, _ in groups[g]], axis=0)
                     gate += mm(a, wg[j * width : (j + 1) * width, fc])
                     up += mm(a, wu[j * width : (j + 1) * width, fc])
                 hid[0:gr, fc] = (gate * jax.nn.sigmoid(gate) * up).astype(BF)
@@ -473,23 +487,20 @@
             lax.fori_loop(lo, hi, tile, 0)
 
     def red_p(g, dy):
-        _, n, r0, _ = groups[g]
-        rs = pl.ds(r0, n * cap)
-        return rc(snd_p.at[dy, rs], rs_p.at[dy, rs], rp_ss.at[g, dy], rp_rs.at[g, dy], me, mate)
-
-    def red_y(g, i, dy):
-        r0 = groups[g][2] + i * cap
-        b = r0 // cap
-        rs = pl.ds(r0, cap)
+        rs = pl.ds(first_of[g] * cap, len(groups[g]) * cap)
+        return rc(snd_p.at[dy, rs], rs_p.at[dy, rs], sem["rp"], rp_rs.at[g, dy], me, mate)
+
+    def red_y(b, dy):
+        rs = pl.ds(b * cap, cap)
         return rc(
-            snd_y.at[dy, rs], rs_y.at[dy, rs], ry_ss.at[b, dy], ry_rs.at[b, dy], me, up_y(dy) * 2 + c
+            snd_y.at[dy, rs], rs_y.at[dy, rs], sem["ry"], ry_rs.at[b, dy - 1], me, up_y(dy) * 2 + c
         )
 
     order = list(range(1, ny)) + [0]
 
     def second(g):
-        _, n, r0, _ = groups[g]
-        gr = n * cap
+        r0 = first_of[g] * cap
+        gr = len(groups[g]) * cap
 
         def down(dy, core):
             col = up_y(dy) * 2 + core
@@ -502,96 +513,118 @@
             for dy in order:
                 own[dy, r0 : r0 + gr] = down(dy, c)
 
-    def reduce_p(g):
-        _, n, r0, _ = groups[g]
-        with NS(f"reduce_p{g}"):
-            for dy in order:
+    def reduce_wait(g):
+        with NS(f"reduce_wait{g}"):
+            for dy in range(1, ny):
                 red_p(g, dy).wait_recv()
-                for i in range(n):
-                    rr = slice(r0 + i * cap, r0 + (i + 1) * cap)
-                    total = own[dy, rr] + rs_p[dy, rr].astype(F32)
-                    if dy:
-                        snd_y[dy, rr] = total.astype(BF)
-                        red_y(g, i, dy).start()
-                    else:
-                        own[0, rr] = total
+
+    def reduce_y(g, i):
+        b = first_of[g] + i
+        rr = slice(b * cap, (b + 1) * cap)
+        with NS(f"reduce_y{g}"):
+            for dy in range(1, ny):
+                snd_y[dy, rr] = (own[dy, rr] + rs_p[dy, rr].astype(F32)).astype(BF)
+                red_y(b, dy).start()
+
+    def reduce_all(g):
+        reduce_wait(g)
+        for i in range(len(groups[g])):
+            reduce_y(g, i)
 
     def back(g, i):
-        base, _, r0, is_near = groups[g]
-        b = r0 // cap + i
-        p = base + i
+        p, is_near = groups[g][i]
+        b = first_of[g] + i
         dest = peer(p) if is_near else peer_dyn(p)
-        return rc(fin.at[b], ret.at[p], b_ss.at[b], b_rs.at[p], dest, t)
-
-    def give_back(g):
-        _, n, r0, _ = groups[g]
+        return rc(fin.at[b], ret.at[p], sem["back"], b_rs.at[p], dest, t)
+
+    def give_wait(g):
+        with NS(f"give_wait{g}"):
+            red_p(g, 0).wait_recv()
+
+    def give_back(g, i):
+        b = first_of[g] + i
+        rr = slice(b * cap, (b + 1) * cap)
         with NS(f"give_back{g}"):
-            for i in range(n):
-                rr = slice(r0 + i * cap, r0 + (i + 1) * cap)
-                total = own[0, rr]
-                for dy in range(1, ny):
-                    red_y(g, i, dy).wait_recv()
-                    total += rs_y[dy, rr].astype(F32)
-                if g == 0 and i == 0:
-                    ret[0] = total.astype(BF)
-                else:
-                    fin[r0 // cap + i] = total.astype(BF)
-                    back(g, i).start()
+            total = own[0, rr] + rs_p[0, rr].astype(F32)
+            for dy in range(1, ny):
+                red_y(b, dy).wait_recv()
+                total += rs_y[dy, rr].astype(F32)
+            if b == 0:
+                ret[0] = total.astype(BF)
+            else:
+                fin[b] = total.astype(BF)
+                back(g, i).start()
+
+    def give_all(g):
+        give_wait(g)
+        for i in range(len(groups[g])):
+            give_back(g, i)
 
     def back_in(p):
-        return rc(fin.at[p], ret.at[p], b_ss.at[p], b_rs.at[p], me, mate)
-
-    def far_taken(g):
-        for i in range(gf):
-            take_far(g, i)
-
-    def far_relayed(g):
-        for i in range(gf):
-            relay_far(g, i)
+        return rc(fin.at[p], ret.at[p], sem["back"], b_rs.at[p], me, mate)
 
     def chain_at(lo, hi):
         with NS(f"chain{lo}"):
             for s in range(lo, min(hi, nz)):
                 chain(s)
 
+    nl = len(far_of(2))
     for p in range(1, gn):
         take_near(p)
+    take_far(1, 0, hf)
     with NS("loads"):
         for load in loads[:3]:
             load.wait()
     arrived(0)
-    first(0, lambda: take_far(1, 0))
-    for i in range(1, gf):
-        take_far(1, i)
+    first(0)
+    take_far(1, hf)
     second(0)
+    reduce_wait(0)
+    reduce_y(0, 0)
+    relay_far(1, 0, hf)
     with NS("pair_states"):
         pair_states()
-    far_relayed(1)
-    reduce_p(0)
+    near_send(near - 1)
+    relay_far(1, hf)
+    for i in range(1, gn):
+        reduce_y(0, i)
+    take_far(2)
     arrived(1)
-    first(1)
+    first(1, lambda: chain_at(1, 2))
     for p in range(gn, near):
         take_near(p)
-    far_taken(3)
+    take_far(3)
     second(1)
-    chain_at(1, 2)
-    give_back(0)
-    reduce_p(1)
+    relay_far(2)
+    reduce_all(1)
+    chain_at(2, 3)
+    give_all(0)
     arrived(2)
-    first(2)
-    far_relayed(3)
+    first(2, lambda: relay_far(3))
+    chain_at(3, nz)
+    mix_close(0, 1)
+    give_wait(1)
+    for i in range(hf):
+        give_back(1, i)
     second(2)
-    chain_at(2, 3)
-    reduce_p(2)
+    reduce_wait(2)
+    for i in range(nl + 1):
+        reduce_y(2, i)
+    for i in range(hf, gf):
+        give_back(1, i)
     arrived(3)
     first(3)
-    give_back(1)
     second(3)
-    chain_at(3, nz)
-    reduce_p(3)
-    mix_close()
-    give_back(2)
-    give_back(3)
+    reduce_all(3)
+    for i in range(nl + 1, len(groups[2])):
+        reduce_y(2, i)
+    mix_close(1)
+    give_wait(2)
+    for i in range(nl + 1):
+        give_back(2, i)
+    give_all(3)
+    for i in range(nl + 1, len(groups[2])):
+        give_back(2, i)
     ho_relay()
     loads[3].wait()
     project()
@@ -609,31 +642,22 @@
         pltpu.make_async_copy(moe_ref, moe_hbm, out_sem.at[1]).start()
 
     with NS("drain"):
-        for p in range(1, ep):
-            a2a(p).wait_send()
-        for g, (base, n, r0, is_near) in enumerate(groups):
-            for i in range(n):
-                if g or i:
-                    back(g, i).wait_send()
-                for dy in range(1, ny):
-                    red_y(g, i, dy).wait_send()
-                if is_near:
-                    near_p(base + i).wait_send()
-                else:
-                    for dy in range(ny):
-                        gat_p(base + i, dy).wait_send()
-                        if dy:
-                            gat_y(base + i, dy).wait_send()
-            for dy in range(ny):
-                red_p(g, dy).wait_send()
-        for h in range(heads):
-            state_x(h).wait_send()
-            pl.when(zi + 1 < nz)(lambda h=h: chain_copy(h).wait_send())
-        for p in range(hpn):
-            for dy in range(ny):
-                ho_p(p, dy).wait_send()
-                if dy:
-                    ho_y(p, dy).wait_send()
+        sent = {
+            "near": dispn.at[:, 1:near],
+            "far": dispf,
+            "gn": dispn,
+            "gy": snd_y.at[1:ny, 0 : far * cap],
+            "gp": snd_y.at[:, 0 : far * cap],
+            "rp": snd_p,
+            "ry": snd_y.at[1:ny],
+            "back": fin.at[1:ep],
+            "kx": kx_s,
+            "hy": ho.at[1:ny, 0],
+            "hp": ho.at[:, 0],
+        }
+        for kind, r in sent.items():
+            rc(r, r, sem[kind], b_rs.at[0], me, mate).wait_send()
+        pl.when(zi + 1 < nz)(lambda: rc(kc_s, kc_s, sem["kc"], b_rs.at[0], me, mate).wait_send())
         pltpu.make_async_copy(mixed_ref, mixed_hbm, out_sem.at[0]).wait()
         pltpu.make_async_copy(moe_ref, moe_hbm, out_sem.at[1]).wait()
 
@@ -669,7 +693,7 @@
     hpn = max(1, heads // 2)
     fu = wg.shape[2]
     slots = ep * cap
-    gmax = max(near // 2, (ep - near) // 2) * cap
+    gmax = max(near // 2, (ep - near) // 2) * cap + near // 2 * cap
     vm = pltpu.VMEM
     dma = pltpu.SemaphoreType.DMA
     operands = (q, fi, v, og, ds.T, ff[None, :], hg[None, :], x, mg[None, :], rt.T, rw.T)
@@ -705,25 +729,18 @@
         dma((len(operands),)),
         dma((2,)),
         dma((4,)),
-        dma((ep,)),
-        dma((ep,)),
-        dma((ny, ep)),
-        dma((ny, ep)),
-        dma((ny, ep)),
-        dma((ny, ep)),
+        dma((12,)),
+        dma((near, ny)),
+        dma((ep - near,)),
+        dma((near, ny)),
+        dma((ny - 1, ep - near)),
+        dma((ny, ep - near)),
         dma((4, ny)),
-        dma((4, ny)),
-        dma((ep, ny)),
-        dma((ep, ny)),
-        dma((ep,)),
+        dma((ep, ny - 1)),
         dma((ep,)),
         dma((heads,)),
         dma((heads,)),
-        dma((heads,)),
-        dma((heads,)),
-        dma((hpn, ny)),
-        dma((hpn, ny)),
-        dma((hpn, ny)),
+        dma((hpn, ny - 1)),
         dma((hpn, ny)),
     ]
     out = jax.ShapeDtypeStruct((rows, width), BF)

time: 53.7 us -> 52.2 us (0.972)
  Pallas kernels: 52.5 us -> 51.3 us
    pallas_call x1, Pallas kernels: 50.7 us -> 49.6 us  [body(): pl.pallas_call(functools.partial(kernel, (ep, tp, cap, near)), out_shape=...]
where the time goes in v2:
time: 52.2 us; the launch traced here: 52 us
  Pallas kernels  51.3 us (98%)
  between operations  0.64 us (1%)
    pallas_call x1, Pallas kernels, body(): pl.pallas_call(functools.partial(kernel, (ep, tp, cap, near)), out_shape=...  49.6 us
    pallas_call x1, Pallas kernels, body(): pl.pallas_call(emit, out_shape=(out, out), in_specs=[in_any] * 2, out_spe...  1.77 us

profile of v2, /device:TPU:0, one launch (start us, length us, event | category | flops | bytes accessed | tf_op | source)
XLA Modules:
  0.0 52.0 jit_solution(6501539410705005823)
XLA Ops:
  0.6 49.6 %shard_map.158 = (bf16[256,512]{1,0:T(8,128)(2,1)}, bf16[256,512]{1,0:T(8,128)(2,1)}) custom-call(bf16[256,512]{1,0:T(8,128)(2,1)} %q_hbm.1, bf16[256,512]{1,0:T(8,128)(2,1)} %fi_hbm.1, bf16[256,512]{1,0:T(8,128)(2,1)} %v_hbm.1, bf16[256,512]{1,0:T(8,128)(2,1)} %og_hbm.1, f32[4,256]{1,0:T(4,128)} %bitcast.7, f32[1,512]{1,0:T(1,128)} %bitcast.8, ...), custom_call_target="tpu_custom_call" | custom-call | tf_op jit(solution)/shard_map/pallas_call | solution.py:748
  50.2 1.8 %emit.1 = (bf16[256,512]{1,0:T(8,128)(2,1)}, bf16[256,512]{1,0:T(8,128)(2,1)}) custom-call(bf16[256,512]{1,0:T(8,128)(2,1)} %get-tuple-element.4.a_ref, bf16[256,512]{1,0:T(8,128)(2,1)} %get-tuple-element.5.b_ref), custom_call_target="tpu_custom_call" | custom-call | tf_op jit(solution)/shard_map/emit/pallas_call | solution.py:758

commit v3 on v2

--- a/solution.py
+++ b/solution.py
@@ -80,6 +80,8 @@
     intra,
     qdec,
     ho,
+    proj,
+    moe_part,
     in_sem,
     out_sem,
     w_sem,
@@ -185,9 +187,10 @@
     hf = gf // 2
     groups = [
         [(p, True) for p in range(gn)],
-        [(p, False) for p in early],
-        [(p, False) for p in late[:hf]] + [(p, True) for p in range(gn, near)],
-        [(p, False) for p in late[hf:]],
+        [(p, False) for p in early[:hf]],
+        [(p, False) for p in early[hf:]],
+        [(p, False) for p in late[:hf]] + [(p, True) for p in range(gn, gn + gn // 2)],
+        [(p, False) for p in late[hf:]] + [(p, True) for p in range(gn + gn // 2, near)],
     ]
     first_of = [sum(len(g) for g in groups[:i]) for i in range(len(groups))]
 
@@ -301,17 +304,23 @@
             return (x_ref[:, cols].astype(F32) * inv * mg_ref[:, cols]).astype(BF)
 
     nr = near * cap
-    with NS("disp_near"):
+
+    def near_rows(lo, hi):
         for yy in range(ny):
-            out = mm(pick[0:nr], normed(yy)).astype(BF).reshape(near, cap, width)
-            dispn[yy] = out
-            xs[yy, c, 0] = out[0]
-    with NS("bar"):
-        pl.semaphore_wait(barrier, ep - 1 + ny)
+            out = mm(pick[lo * cap : hi * cap], rows_of[yy]).astype(BF).reshape(hi - lo, cap, width)
+            dispn[yy, lo:hi] = out
+            if lo == 0:
+                xs[yy, c, 0] = out[0]
+
     def near_send(p):
         for yy in range(ny):
             near_a2a(p, yy).start()
 
+    with NS("disp_near"):
+        rows_of = [normed(yy) for yy in range(ny)]
+        near_rows(0, gn)
+    with NS("bar"):
+        pl.semaphore_wait(barrier, ep - 1 + ny)
     for p in range(1, gn):
         near_send(p)
     with NS("disp_far"):
@@ -319,8 +328,8 @@
     for i in range(gf):
         for p in (early[i], late[i]):
             far_a2a(p).start()
-    for p in range(gn, near - 1):
-        near_send(p)
+    with NS("disp_near"):
+        near_rows(gn, near)
     take_near(0)
 
     causal = i_r >= i_c
@@ -436,26 +445,28 @@
                     ho_y(p, dy).start()
                 ho_p(p, 0).start()
 
-    def ho_relay():
+    def ho_relay(p):
         with NS("ho_relay"):
-            for p in range(hpn):
-                for dy in range(1, ny):
-                    ho_y_in(p, dy).wait_recv()
-                    ho_p(p, dy).start()
-
-    def project():
+            for dy in range(1, ny):
+                ho_y_in(p, dy).wait_recv()
+                ho_p(p, dy).start()
+
+    def project(lo, hi):
         with NS("ho_wait"):
-            for p in range(hpn):
+            for p in range(lo, hi):
                 for dy in range(ny):
                     ho_p_in(p, dy).wait_recv()
         with NS("proj"):
-            acc = jnp.zeros(mixed_ref.shape, F32)
+            acc = proj[...] if lo else jnp.zeros(proj.shape, F32)
             for j in range(tp):
-                for p in range(hpn):
-                    k0 = j * hw + p * cw
-                    acc += mm(ho[j // 2, j % 2, p], wm[k0 : k0 + cw, :])
-            mixed_ref[...] = acc.astype(BF)
-            pltpu.make_async_copy(mixed_ref, mixed_hbm, out_sem.at[0]).start()
+                k0 = j * hw + lo * cw
+                a = jnp.concatenate([ho[j // 2, j % 2, p] for p in range(lo, hi)], axis=1)
+                acc += mm(a, wm[k0 : k0 + (hi - lo) * cw, :])
+            if hi < hpn:
+                proj[...] = acc
+            else:
+                mixed_ref[...] = acc.astype(BF)
+                pltpu.make_async_copy(mixed_ref, mixed_hbm, out_sem.at[0]).start()
 
     ft = min(256, hidden_units)
 
@@ -498,7 +509,7 @@
 
     order = list(range(1, ny)) + [0]
 
-    def second(g):
+    def second(g, between=None):
         r0 = first_of[g] * cap
         gr = len(groups[g]) * cap
 
@@ -510,6 +521,9 @@
             for dy in order:
                 snd_p[dy, r0 : r0 + gr] = down(dy, 1 - c).astype(BF)
                 red_p(g, dy).start()
+        if between is not None:
+            between()
+        with NS(f"second{g}"):
             for dy in order:
                 own[dy, r0 : r0 + gr] = down(dy, c)
 
@@ -568,76 +582,84 @@
             for s in range(lo, min(hi, nz)):
                 chain(s)
 
-    nl = len(far_of(2))
+    half = gn + gn // 2
+    step = max(1, hpn // 2)
     for p in range(1, gn):
         take_near(p)
-    take_far(1, 0, hf)
+    take_far(1)
     with NS("loads"):
         for load in loads[:3]:
             load.wait()
     arrived(0)
     first(0)
-    take_far(1, hf)
-    second(0)
+
+    def between_0():
+        take_far(2)
+        with NS("pair_states"):
+            pair_states()
+        for p in range(gn, near):
+            near_send(p)
+
+    second(0, between_0)
     reduce_wait(0)
     reduce_y(0, 0)
-    relay_far(1, 0, hf)
-    with NS("pair_states"):
-        pair_states()
-    near_send(near - 1)
-    relay_far(1, hf)
+    relay_far(1)
     for i in range(1, gn):
         reduce_y(0, i)
-    take_far(2)
+    take_far(3)
     arrived(1)
-    first(1, lambda: chain_at(1, 2))
-    for p in range(gn, near):
+    first(1)
+    relay_far(2)
+    second(1)
+    reduce_all(1)
+    chain_at(1, 2)
+    arrived(2)
+    first(2)
+    take_far(4)
+    second(2)
+    for p in range(gn, half):
         take_near(p)
-    take_far(3)
-    second(1)
-    relay_far(2)
-    reduce_all(1)
+    relay_far(3)
+    reduce_all(2)
     chain_at(2, 3)
+    pl.when(zi <= 2)(lambda: mix_close(0, step))
     give_all(0)
-    arrived(2)
-    first(2, lambda: relay_far(3))
-    chain_at(3, nz)
-    mix_close(0, 1)
-    give_wait(1)
-    for i in range(hf):
-        give_back(1, i)
-    second(2)
-    reduce_wait(2)
-    for i in range(nl + 1):
-        reduce_y(2, i)
-    for i in range(hf, gf):
-        give_back(1, i)
     arrived(3)
-    first(3)
+
+    def between_3():
+        for p in range(half, near):
+            take_near(p)
+
+    first(3, between_3)
+    give_all(1)
+    relay_far(4)
     second(3)
     reduce_all(3)
-    for i in range(nl + 1, len(groups[2])):
-        reduce_y(2, i)
-    mix_close(1)
-    give_wait(2)
-    for i in range(nl + 1):
-        give_back(2, i)
+    give_all(2)
+    chain_at(3, nz)
+    arrived(4)
+    first(4)
+    second(4)
+    reduce_all(4)
+    pl.when(zi > 2)(lambda: mix_close(0, step))
+    mix_close(step)
     give_all(3)
-    for i in range(nl + 1, len(groups[2])):
-        give_back(2, i)
-    ho_relay()
+    give_all(4)
     loads[3].wait()
-    project()
+    for lo in range(0, hpn, step):
+        for p in range(lo, lo + step):
+            ho_relay(p)
+        project(lo, lo + step)
     with NS("near_back"):
         for p in range(1, near):
             back_in(p).wait_recv()
     with NS("comb_near"):
-        res = mm(wpn[...], ret[0:near].reshape(nr, width))
+        moe_part[...] = mm(wpn[...], ret[0:near].reshape(nr, width))
     with NS("far_back"):
         for p in range(near, ep):
             back_in(p).wait_recv()
     with NS("comb_far"):
-        res += mm(wpf[...], ret[near:].reshape(slots - nr, width))
+        res = moe_part[...] + mm(wpf[...], ret[near:].reshape(slots - nr, width))
         moe_ref[...] = res.astype(BF)
         pltpu.make_async_copy(moe_ref, moe_hbm, out_sem.at[1]).start()
 
@@ -690,7 +712,7 @@
     heads = ds.shape[1]
     hs = hg.shape[0]
     hw = q.shape[1]
-    hpn = max(1, heads // 2)
+    hpn = heads
     fu = wg.shape[2]
     slots = ep * cap
     gmax = max(near // 2, (ep - near) // 2) * cap + near // 2 * cap
@@ -726,6 +748,8 @@
         vm((rows, hw), F32),
         vm((rows, hw), BF),
         vm((ny, 2, hpn, rows, hw // hpn), BF),
+        vm((rows, width), F32),
+        vm((rows, width), F32),
         dma((len(operands),)),
         dma((2,)),
         dma((4,)),
@@ -735,7 +759,7 @@
         dma((near, ny)),
         dma((ny - 1, ep - near)),
         dma((ny, ep - near)),
-        dma((4, ny)),
+        dma((5, ny)),
         dma((ep, ny - 1)),
         dma((ep,)),
         dma((heads,)),

time: 52.2 us -> 49.9 us (0.956); the launches traced: 52 us -> 49.1 us
  Pallas kernels: 51.3 us -> 48.4 us
    pallas_call x1, Pallas kernels: 49.6 us -> 46.6 us  [body(): pl.pallas_call(functools.partial(kernel, (ep, tp, cap, near)), out_shape=...]
where the time goes in v3:
time: 49.9 us; the launch traced here: 49.1 us
  Pallas kernels  48.4 us (97%)
  between operations  0.64 us (1%)
    pallas_call x1, Pallas kernels, body(): pl.pallas_call(functools.partial(kernel, (ep, tp, cap, near)), out_shape=...  46.6 us
    pallas_call x1, Pallas kernels, body(): pl.pallas_call(emit, out_shape=(out, out), in_specs=[in_any] * 2, out_spe...  1.77 us

profile of v3, /device:TPU:0, one launch (start us, length us, event | category | flops | bytes accessed | tf_op | source)
XLA Modules:
  0.0 49.1 jit_solution(2636866720442264658)
XLA Ops:
  0.6 46.6 %shard_map.158 = (bf16[256,512]{1,0:T(8,128)(2,1)}, bf16[256,512]{1,0:T(8,128)(2,1)}) custom-call(bf16[256,512]{1,0:T(8,128)(2,1)} %q_hbm.1, bf16[256,512]{1,0:T(8,128)(2,1)} %fi_hbm.1, bf16[256,512]{1,0:T(8,128)(2,1)} %v_hbm.1, bf16[256,512]{1,0:T(8,128)(2,1)} %og_hbm.1, f32[4,256]{1,0:T(4,128)} %bitcast.7, f32[1,512]{1,0:T(1,128)} %bitcast.8, ...), custom_call_target="tpu_custom_call" | custom-call | tf_op jit(solution)/shard_map/pallas_call | solution.py:772
  47.3 1.8 %emit.1 = (bf16[256,512]{1,0:T(8,128)(2,1)}, bf16[256,512]{1,0:T(8,128)(2,1)}) custom-call(bf16[256,512]{1,0:T(8,128)(2,1)} %get-tuple-element.4.a_ref, bf16[256,512]{1,0:T(8,128)(2,1)} %get-tuple-element.5.b_ref), custom_call_target="tpu_custom_call" | custom-call | tf_op jit(solution)/shard_map/emit/pallas_call | solution.py:782

commit v4 on v3

--- a/solution.py
+++ b/solution.py
@@ -626,12 +626,10 @@
     give_all(0)
     arrived(3)
 
-    def between_3():
-        for p in range(half, near):
-            take_near(p)
-
-    first(3, between_3)
+    first(3)
     give_all(1)
+    for p in range(half, near):
+        take_near(p)
     relay_far(4)
     second(3)
     reduce_all(3)
@@ -659,9 +657,11 @@
         for p in range(near, ep):
             back_in(p).wait_recv()
     with NS("comb_far"):
-        res = moe_part[...] + mm(wpf[...], ret[near:].reshape(slots - nr, width))
-        moe_ref[...] = res.astype(BF)
-        pltpu.make_async_copy(moe_ref, moe_hbm, out_sem.at[1]).start()
+        far_back = ret[near:].reshape(slots - nr, width)
+        for i in range(2):
+            rh = slice(i * rows // 2, (i + 1) * rows // 2)
+            moe_ref[rh] = (moe_part[rh] + mm(wpf[rh], far_back)).astype(BF)
+            pltpu.make_async_copy(moe_ref.at[rh], moe_hbm.at[rh], out_sem.at[1 + i]).start()
 
     with NS("drain"):
         sent = {
@@ -681,7 +681,9 @@
             rc(r, r, sem[kind], b_rs.at[0], me, mate).wait_send()
         pl.when(zi + 1 < nz)(lambda: rc(kc_s, kc_s, sem["kc"], b_rs.at[0], me, mate).wait_send())
         pltpu.make_async_copy(mixed_ref, mixed_hbm, out_sem.at[0]).wait()
-        pltpu.make_async_copy(moe_ref, moe_hbm, out_sem.at[1]).wait()
+        for i in range(2):
+            rh = slice(i * rows // 2, (i + 1) * rows // 2)
+            pltpu.make_async_copy(moe_ref.at[rh], moe_hbm.at[rh], out_sem.at[1 + i]).wait()
 
 
 def emit(a_ref, b_ref, a_out, b_out, held, sem):
@@ -751,7 +753,7 @@
         vm((rows, width), F32),
         vm((rows, width), F32),
         dma((len(operands),)),
-        dma((2,)),
+        dma((3,)),
         dma((4,)),
         dma((12,)),
         dma((near, ny)),

time: 49.9 us -> 49.8 us (level)
  no operation moved by 1% of the time
where the time goes in v4:
time: 49.8 us; the launch traced here: 49 us
  Pallas kernels  48.4 us (97%)
  between operations  0.64 us (1%)
    pallas_call x1, Pallas kernels, body(): pl.pallas_call(functools.partial(kernel, (ep, tp, cap, near)), out_shape=...  46.6 us
    pallas_call x1, Pallas kernels, body(): pl.pallas_call(emit, out_shape=(out, out), in_specs=[in_any] * 2, out_spe...  1.77 us

profile of v4, /device:TPU:0, one launch (start us, length us, event | category | flops | bytes accessed | tf_op | source)
XLA Modules:
  0.0 49.0 jit_solution(9453985131213735051)
XLA Ops:
  0.6 46.6 %shard_map.158 = (bf16[256,512]{1,0:T(8,128)(2,1)}, bf16[256,512]{1,0:T(8,128)(2,1)}) custom-call(bf16[256,512]{1,0:T(8,128)(2,1)} %q_hbm.1, bf16[256,512]{1,0:T(8,128)(2,1)} %fi_hbm.1, bf16[256,512]{1,0:T(8,128)(2,1)} %v_hbm.1, bf16[256,512]{1,0:T(8,128)(2,1)} %og_hbm.1, f32[4,256]{1,0:T(4,128)} %bitcast.7, f32[1,512]{1,0:T(1,128)} %bitcast.8, ...), custom_call_target="tpu_custom_call" | custom-call | tf_op jit(solution)/shard_map/pallas_call | solution.py:774
  47.2 1.8 %emit.1 = (bf16[256,512]{1,0:T(8,128)(2,1)}, bf16[256,512]{1,0:T(8,128)(2,1)}) custom-call(bf16[256,512]{1,0:T(8,128)(2,1)} %get-tuple-element.4.a_ref, bf16[256,512]{1,0:T(8,128)(2,1)} %get-tuple-element.5.b_ref), custom_call_target="tpu_custom_call" | custom-call | tf_op jit(solution)/shard_map/emit/pallas_call | solution.py:784
